TPU v7x, 32 devices: a whole 2x2x4 slice. The times are simulated.
32 devices in a mesh: ep: 8 (over z, x), tp: 4 (over y, core).
Axes of the slice: x: 2, y: 2, z: 4, core: 2. Of those that a mesh axis runs over, the one named last changes fastest.
Arguments:
- residual: bfloat16 [512, 4096], P('ep', 'tp'), may hold values from -64 to 64
- routes: int32 [512, 2], P('ep'), may hold values from 0 to 7, all different within a row; in each aligned block of 64 rows (0 to 63, 64 to 127, ...) at most 32 rows name the same one
- route_weights: float32 [512, 2], P('ep'), may hold values from 0.2 to 1
- state_prev: float32 [512, 2, 64, 64], P('ep', None, 'tp'), may hold values from -6 to 6
- mix_gain: float32 [4096], replicated, may hold values from 0.1 to 1.9
- ffn_gain: float32 [4096], replicated, may hold values from 0.1 to 1.9
- w_in: bfloat16 [4096, 1024], P(None, 'tp'), may hold values from -0.09375 to 0.09375
- decay_rate: float32 [64, 64], P('tp'), may hold values from 0.5 to 8
- rotation: float32 [64, 64], P('tp'), may hold values from 0 to 200
- log_step: float32 [64], P('tp'), may hold values from -3.9 to -1.2
- in_re: float32 [64, 64, 16], P('tp'), may hold values from -1 to 1
- in_im: float32 [64, 64, 16], P('tp'), may hold values from -1 to 1
- read_re: float32 [64, 16, 64], P('tp'), may hold values from -0.5 to 0.5
- read_im: float32 [64, 16, 64], P('tp'), may hold values from -0.5 to 0.5
- skip_gain: float32 [64, 16], P('tp'), may hold values from -4 to 4
- w_glu: bfloat16 [1024, 1024], P(None, 'tp'), may hold values from -0.1875 to 0.1875
- w_out: bfloat16 [1024, 4096], P('tp'), may hold values from -0.1875 to 0.1875
- w_gate: bfloat16 [8, 4096, 5632], P('ep', None, 'tp'), may hold values from -0.09375 to 0.09375
- w_up: bfloat16 [8, 4096, 5632], P('ep', None, 'tp'), may hold values from -0.09375 to 0.09375
- w_down: bfloat16 [8, 5632, 4096], P('ep', 'tp'), may hold values from -0.078125 to 0.078125
Outputs:
- layer_out: bfloat16 [512, 4096], P('ep', 'tp')
- state_next: float32 [512, 2, 64, 64], P('ep', None, 'tp')
Inputs may be any that keep to these rules, and one draw needn't show every extreme that they name: `routes`: each row names 2 different experts. In each aligned block of 64 rows (the rows of one index of ep) no expert is named more than 32 times, a bound that some block reaches.
All inputs are finite; a program needn't handle non-finite values.
Results may differ from a plain program's by a relative error of at most 0.012.
Values may be sent and summed in bfloat16 or wider, within the bound.
A program may use at most 128 MiB of HBM per device.

v0:
```python
import jax
import jax.numpy as jnp
from jax import lax
from jax.sharding import PartitionSpec as P

GROUP_CH = 16
TOPK = 2


epsilon = 1e-06
highest = lax.Precision.HIGHEST


def state_mixer(
    u_in, state_prev, decay_rate, rotation, log_step, in_re, in_im, read_re, read_im, skip_gain
):
    batch_rows = u_in.shape[0]
    groups = decay_rate.shape[0]
    grouped = u_in.astype(jnp.float32).reshape(batch_rows, groups, GROUP_CH)
    step_size = jnp.exp(log_step)[:, None]
    real_part = -decay_rate
    magnitude = jnp.exp(real_part * step_size)
    decay_re = magnitude * jnp.cos(rotation * step_size)
    decay_im = magnitude * jnp.sin(rotation * step_size)
    denominator = real_part * real_part + rotation * rotation
    lift_re = ((decay_re - 1.0) * real_part + decay_im * rotation) / denominator
    lift_im = (decay_im * real_part - (decay_re - 1.0) * rotation) / denominator
    map_re = lift_re[..., None] * in_re - lift_im[..., None] * in_im
    map_im = lift_re[..., None] * in_im + lift_im[..., None] * in_re
    drive_re = jnp.einsum("gph,bgh->bgp", map_re, grouped, precision=highest)
    drive_im = jnp.einsum("gph,bgh->bgp", map_im, grouped, precision=highest)
    old_re = state_prev[:, 0]
    old_im = state_prev[:, 1]
    new_re = decay_re * old_re - decay_im * old_im + drive_re
    new_im = decay_re * old_im + decay_im * old_re + drive_im
    output = (
        jnp.einsum("ghp,bgp->bgh", read_re, new_re, precision=highest)
        - jnp.einsum("ghp,bgp->bgh", read_im, new_im, precision=highest)
        + skip_gain * grouped
    )
    return (jax.nn.gelu(output.reshape(batch_rows, -1)), jnp.stack([new_re, new_im], axis=1))


def per_device(
    residual,
    routes,
    route_weights,
    state_prev,
    mix_gain,
    ffn_gain,
    w_in,
    decay_rate,
    rotation,
    log_step,
    in_re,
    in_im,
    read_re,
    read_im,
    skip_gain,
    w_glu,
    w_out,
    w_gate,
    w_up,
    w_down,
):
    shard_width = residual.shape[1]
    full_width = shard_width * lax.axis_size("tp")
    tp_place = lax.axis_index("tp")
    experts_all = lax.axis_size("ep")
    seq_rows = residual.shape[0]
    capacity = 2 * seq_rows * TOPK // experts_all
    source = residual.astype(jnp.float32)
    squares = lax.psum(jnp.sum(source * source, axis=1), "tp")
    own_gain = lax.dynamic_slice_in_dim(mix_gain, tp_place * shard_width, shard_width)
    scale_rows = lax.rsqrt(squares / full_width + epsilon)[:, None]
    outgoing = (source * scale_rows * own_gain).astype(jnp.bfloat16)
    gathered = lax.all_gather(outgoing, "tp", axis=1, tiled=True)
    u_in = jnp.dot(gathered, w_in, preferred_element_type=jnp.float32).astype(jnp.bfloat16)
    mixer_act, state_next = state_mixer(
        u_in, state_prev, decay_rate, rotation, log_step, in_re, in_im, read_re, read_im, skip_gain
    )
    mixer_bf = mixer_act.astype(jnp.bfloat16)
    all_channels = lax.all_gather(mixer_bf, "tp", axis=1, tiled=True)
    glu_logit = jnp.dot(all_channels, w_glu, preferred_element_type=jnp.float32)
    mixed = (mixer_act * jax.nn.sigmoid(glu_logit)).astype(jnp.bfloat16)
    partial_out = jnp.dot(mixed, w_out, preferred_element_type=jnp.float32)
    branch = lax.psum_scatter(
        partial_out.astype(jnp.bfloat16), "tp", scatter_dimension=1, tiled=True
    ).astype(jnp.float32)
    after_float = (source + branch).astype(jnp.bfloat16).astype(jnp.float32)
    squares_ffn = lax.psum(jnp.sum(after_float * after_float, axis=1), "tp")
    ffn_own = lax.dynamic_slice_in_dim(ffn_gain, tp_place * shard_width, shard_width)
    scale_ffn = lax.rsqrt(squares_ffn / full_width + epsilon)[:, None]
    normed_ffn = (after_float * scale_ffn * ffn_own).astype(jnp.bfloat16)
    flat_routes = routes.reshape(-1)
    onehot = (flat_routes[:, None] == jnp.arange(experts_all, dtype=jnp.int32)).astype(jnp.int32)
    before = jnp.cumsum(onehot, axis=0) - onehot
    slot_index = jnp.sum(before * onehot, axis=1)
    destination = (flat_routes * capacity + slot_index).reshape(seq_rows, TOPK)
    matches = destination[:, :, None] == jnp.arange(experts_all * capacity, dtype=jnp.int32)
    dispatch_map = jnp.sum(matches.astype(jnp.float32), axis=1).astype(jnp.bfloat16)
    combine_map = jnp.sum(jnp.where(matches, route_weights[:, :, None], 0.0), axis=1)
    outbound = jnp.einsum("bj,bd->jd", dispatch_map, normed_ffn, preferred_element_type=jnp.float32)
    outbound = outbound.astype(jnp.bfloat16).reshape(experts_all, capacity, shard_width)
    arrived = lax.all_gather(
        lax.all_to_all(outbound, "ep", split_axis=0, concat_axis=0, tiled=True),
        "tp",
        axis=2,
        tiled=True,
    )
    sources, slots_here, row_width = arrived.shape
    flat_rows = arrived.reshape(sources * slots_here, row_width)
    gate_value = jnp.dot(flat_rows, w_gate[0], preferred_element_type=jnp.float32)
    up_value = jnp.dot(flat_rows, w_up[0], preferred_element_type=jnp.float32)
    hidden = (jax.nn.silu(gate_value) * up_value).astype(jnp.bfloat16)
    partial_sum = jnp.dot(hidden, w_down[0], preferred_element_type=jnp.float32)
    partial_sum = partial_sum.reshape(sources, slots_here, row_width)
    reduced = lax.psum_scatter(
        partial_sum.astype(jnp.bfloat16), "tp", scatter_dimension=2, tiled=True
    )
    came_back = lax.all_to_all(reduced, "ep", split_axis=0, concat_axis=0, tiled=True)
    came_back = came_back.reshape(experts_all * capacity, shard_width).astype(jnp.float32)
    combined = jnp.dot(combine_map, came_back, precision=highest)
    layer_out = (after_float + combined).astype(jnp.bfloat16)
    return (layer_out, state_next)


def solution(mesh):
    return jax.shard_map(
        per_device,
        mesh=mesh,
        in_specs=(
            P("ep", "tp"),
            P("ep", None),
            P("ep", None),
            P("ep", None, "tp", None),
            P(),
            P(),
            P(None, "tp"),
            P("tp", None),
            P("tp", None),
            P("tp"),
            P("tp", None, None),
            P("tp", None, None),
            P("tp", None, None),
            P("tp", None, None),
            P("tp", None),
            P(None, "tp"),
            P("tp", None),
            P("ep", None, "tp"),
            P("ep", None, "tp"),
            P("ep", "tp", None),
        ),
        out_specs=(P("ep", "tp"), P("ep", None, "tp", None)),
        check_vma=False,
    )
```

profile of v0, /device:TPU:0, one launch (start us, length us, event | category | flops | bytes accessed | tf_op | source)
XLA Modules:
  0.0 192.4 jit_solution(10713720667919204251)
XLA Ops:
  8.0 1.0 fusion.25
  9.1 8.4 %psum.14 = f32[64]{0:T(128)S(1)} all-reduce(f32[64]{0:T(128)S(1)} %fusion.25), channel_id=1, replica_groups=mesh['ep'=8,'tp'=4] {'tp'}, use_global_device_ids=true, to_apply=%region_1.0 | all-reduce | flops 64 | bytes 512 | tf_op jit(solution)/shard_map/psum | solution.py:73
  18.2 1.0 fusion.27
  19.2 6.5 %all_gather.9 = bf16[64,4096]{1,0:T(8,128)(2,1)S(1)} all-gather(bf16[64,1024]{1,0:T(8,128)(2,1)S(1)} %fusion.27), channel_id=1, replica_groups=mesh['ep'=8,'tp'=4] {'tp'}, dimensions={1}, use_global_device_ids=true | all-gather | bytes 655360 | tf_op jit(solution)/shard_map/all_gather | solution.py:77
  25.7 2.1 %convolution_convert_fusion.2 = bf16[64,256]{1,0:T(8,128)(2,1)S(1)} fusion(bf16[64,4096]{1,0:T(8,128)(2,1)S(1)} %all_gather.9, bf16[4096,256]{1,0:T(8,128)(2,1)} %param.26), kind=kOutput, calls=%fused_computation.26 | convolution fusion | flops 134234112 | bytes 2654208 | tf_op jit(solution)/shard_map/dot_general | solution.py:78
  27.9 1.3 fusion.62
  30.7 0.9 fusion.63
  31.7 0.9 fusion.19
  32.7 5.4 %all_gather.10 = bf16[64,1024]{1,0:T(8,128)(2,1)S(1)} all-gather(bf16[64,256]{1,0:T(8,128)(2,1)S(1)} %fusion.56), channel_id=1, replica_groups=mesh['ep'=8,'tp'=4] {'tp'}, dimensions={1}, use_global_device_ids=true | all-gather | bytes 163840 | tf_op jit(solution)/shard_map/all_gather | solution.py:83
  38.2 2.7 %convolution_convert_fusion = bf16[64,4096]{1,0:T(8,128)(2,1)} fusion(bf16[256,4096]{1,0:T(8,128)(2,1)S(1)} %copy-done, bf16[64,1024]{1,0:T(8,128)(2,1)S(1)} %all_gather.10, bf16[1024,256]{1,0:T(8,128)(2,1)} %param.35, f32[64,256]{1,0:T(8,128)S(1)} %copy.60), kind=kOutput, calls=%fused_computation.7 | convolution fusion | flops 168247296 | bytes 3342336 | tf_op jit(solution)/shard_map/dot_general | solution.py:86
  42.0 21.7 %reduce-scatter.3.cloned.1.call-done = bf16[64,1024]{1,0:T(8,128)(2,1)} async-done(((bf16[64,4096]{1,0:T(8,128)(2,1)}), bf16[64,1024]{1,0:T(8,128)(2,1)}) %reduce-scatter.3.cloned.1.call-update) | async-done | bytes 131088 | tf_op jit(solution)/shard_map/reduce_scatter | solution.py:87
  63.6 1.0 fusion.29
  64.7 5.8 %psum.15 = f32[64]{0:T(128)S(1)} all-reduce(f32[64]{0:T(128)S(1)} %fusion.29), channel_id=1, replica_groups=mesh['ep'=8,'tp'=4] {'tp'}, use_global_device_ids=true, to_apply=%region_8.9 | all-reduce | flops 64 | bytes 512 | tf_op jit(solution)/shard_map/psum | solution.py:91
  70.5 1.2 convolution_convert_fusion.1
  71.7 19.8 %all_to_all.10 = bf16[8,32,1024]{2,1,0:T(8,128)(2,1)} all-to-all(bf16[8,32,1024]{2,1,0:T(8,128)(2,1)S(1)} %bitcast.67), channel_id=1, replica_groups=mesh['ep'=8,'tp'=4] {'ep'}, dimensions={0} | all-to-all | bytes 1048576 | tf_op jit(solution)/shard_map/all_to_all | solution.py:106
  91.6 20.8 %all-gather.2.cloned.1.call-done = bf16[8,32,4096]{2,1,0:T(8,128)(2,1)} async-done(((bf16[8,32,1024]{2,1,0:T(8,128)(2,1)}), bf16[8,32,4096]{2,1,0:T(8,128)(2,1)}) %all-gather.2.cloned.1.call-update) | async-done | bytes 2097168 | tf_op jit(solution)/shard_map/all_gather | solution.py:105
  112.4 7.4 %fusion.4 = f32[256,1408]{1,0:T(8,128)S(1)} fusion(bf16[256,4096]{1,0:T(8,128)(2,1)} %bitcast.74, bf16[1,4096,1408]{2,1,0:T(8,128)(2,1)} %param.37), kind=kOutput, calls=%fused_computation.4 | convolution fusion | flops 2952790016 | bytes 15073280 | tf_op jit(solution)/shard_map/dot_general | solution.py:113
  119.9 8.0 %fusion.12 = bf16[256,1408]{1,0:T(8,128)(2,1)S(1)} fusion(bf16[256,4096]{1,0:T(8,128)(2,1)S(1)} %bitcast.75, bf16[1,4096,1408]{2,1,0:T(8,128)(2,1)} %param.38, f32[256,1408]{1,0:T(8,128)S(1)} %fusion.4), kind=kOutput, calls=%fused_computation.9 | convolution fusion | flops 2954952704 | bytes 15794176 | tf_op jit(solution)/shard_map/dot_general | solution.py:114
  127.9 4.6 %fusion.6 = bf16[8,32,4096]{2,1,0:T(8,128)(2,1)} fusion(bf16[8,32,1408]{2,1,0:T(8,128)(2,1)S(1)} %bitcast.76, bf16[1,1408,4096]{2,1,0:T(8,128)(2,1)S(1)} %bitcast.73), kind=kOutput, calls=%fused_computation.6 | convolution fusion | flops 2953838592 | bytes 14352384 | tf_op jit(solution)/shard_map/dot_general | solution.py:116
  132.6 31.3 %reduce-scatter.5.cloned.1.call-done = bf16[8,32,1024]{2,1,0:T(8,128)(2,1)} async-done(((bf16[8,32,4096]{2,1,0:T(8,128)(2,1)}), bf16[8,32,1024]{2,1,0:T(8,128)(2,1)}) %reduce-scatter.5.cloned.1.call-update) | async-done | bytes 524304 | tf_op jit(solution)/shard_map/reduce_scatter | solution.py:118
  163.9 5.5 %all-to-all-start.1 = ((bf16[8,32,1024]{2,1,0:T(8,128)(2,1)}), bf16[8,32,1024]{2,1,0:T(8,128)(2,1)}, u32[]{:S(2)}, u32[]{:S(2)}) async-start(bf16[8,32,1024]{2,1,0:T(8,128)(2,1)} %reduce-scatter.5.cloned.1.call-done), calls=%async_computation.3 | async-start | bytes 1048576 | tf_op jit(solution)/shard_map/all_to_all | solution.py:121
  169.5 1.6 copy.63
  171.1 12.7 %all-to-all-done.1 = bf16[8,32,1024]{2,1,0:T(8,128)(2,1)} async-done(((bf16[8,32,1024]{2,1,0:T(8,128)(2,1)}), bf16[8,32,1024]{2,1,0:T(8,128)(2,1)}, u32[]{:S(2)}, u32[]{:S(2)}) %all-to-all-start.1) | async-done | bytes 524320 | tf_op jit(solution)/shard_map/all_to_all | solution.py:121
  183.8 2.1 %fusion.17 = bf16[64,1024]{1,0:T(8,128)(2,1)} fusion(f32[64,256]{1,0:T(8,128)S(1)} %get-tuple-element.11, bf16[256,1024]{1,0:T(8,128)(2,1)} %bitcast.14, bf16[64,1024]{1,0:T(8,128)(2,1)S(1)} %copy-done.2, bf16[64,1024]{1,0:T(8,128)(2,1)S(1)} %copy-done.1), kind=kOutput, calls=%fused_computation.16 | convolution fusion | flops 201785344 | bytes 983040 | tf_op jit(solution)/shard_map/dot_general | solution.py:123
  (61 shorter events, 4.5 us)
Async XLA Ops:
  7.2 31.0 %copy-start = (bf16[256,4096]{1,0:T(8,128)(2,1)S(1)}, bf16[256,4096]{1,0:T(8,128)(2,1)}, u32[]{:S(2)}) copy-start(bf16[256,4096]{1,0:T(8,128)(2,1)} %param.36) | copy-start | bytes 6291460
  7.2 56.5 %reduce-scatter.3.cloned.1.call-start = ((), (), s32[]{:S(2)}) async-start(), calls=%async_computation.4 | async-start | bytes 655360 | tf_op jit(solution)/shard_map/reduce_scatter | solution.py:87
  25.7 3.5 %copy-start.8 = (f32[16,64]{1,0:T(8,128)S(1)}, f32[16,64]{1,0:T(8,128)}, u32[]{:S(2)}) copy-start(f32[16,64]{1,0:T(8,128)} %param.28) | copy-start | bytes 12292
  25.7 3.5 %copy-start.9 = (f32[16,64]{1,0:T(8,128)S(1)}, f32[16,64]{1,0:T(8,128)}, u32[]{:S(2)}) copy-start(f32[16,64]{1,0:T(8,128)} %param.27) | copy-start | bytes 12292
  25.7 3.7 %copy-start.3 = (f32[16,64,16]{1,2,0:T(8,128)S(1)}, f32[16,64,16]{1,2,0:T(8,128)}, u32[]{:S(2)}) copy-start(f32[16,64,16]{1,2,0:T(8,128)} %param.31) | copy-start | bytes 196612
  25.7 3.7 %copy-start.4 = (f32[16,64,16]{1,2,0:T(8,128)S(1)}, f32[16,64,16]{1,2,0:T(8,128)}, u32[]{:S(2)}) copy-start(f32[16,64,16]{1,2,0:T(8,128)} %param.30) | copy-start | bytes 196612
  29.2 1.5 copy-start.6
  29.4 2.3 %copy-start.5 = (f32[16,16,64]{2,1,0:T(8,128)S(1)}, f32[16,16,64]{2,1,0:T(8,128)}, u32[]{:S(2)}) copy-start(f32[16,16,64]{2,1,0:T(8,128)} %param.33) | copy-start | bytes 196612
  29.4 2.3 %copy-start.7 = (f32[16,16]{1,0:T(8,128)S(1)}, f32[16,16]{1,0:T(8,128)}, u32[]{:S(2)}) copy-start(f32[16,16]{1,0:T(8,128)} %param.34) | copy-start | bytes 3076
  32.7 8.2 %copy-start.10 = (s32[64,2]{0,1:T(2,128)S(1)}, s32[64,2]{0,1:T(2,128)}, u32[]{:S(2)}) copy-start(s32[64,2]{0,1:T(2,128)} %param.21) | copy-start | bytes 1540
  38.2 3.7 %copy-start.11 = (f32[64,2]{0,1:T(2,128)S(1)}, f32[64,2]{0,1:T(2,128)}, u32[]{:S(2)}) copy-start(f32[64,2]{0,1:T(2,128)} %param.22) | copy-start | bytes 1540
  38.2 25.5 %copy-start.1 = (bf16[64,1024]{1,0:T(8,128)(2,1)S(1)}, bf16[64,1024]{1,0:T(8,128)(2,1)}, u32[]{:S(2)}) copy-start(bf16[64,1024]{1,0:T(8,128)(2,1)} %param.20) | copy-start | bytes 393220
  38.2 32.3 %dynamic-slice-start = ((f32[4096]{0:T(1024)}, s32[]{:T(128)}), f32[1024]{0:T(1024)S(1)}, s32[]{:S(2)}) async-start(f32[4096]{0:T(1024)} %param.25, s32[]{:T(128)} %select_n.8), calls=%async_computation.7 | async-start | bytes 8704 | tf_op jit(solution)/shard_map/dynamic_slice | solution.py:92
  40.9 71.6 %all-gather.2.cloned.1.call-start = ((), (), s32[]{:S(2)}) async-start(), calls=%async_computation.5 | async-start | bytes 2621440 | tf_op jit(solution)/shard_map/all_gather | solution.py:105
  91.6 72.3 %reduce-scatter.5.cloned.1.call-start = ((), (), s32[]{:S(2)}) async-start(), calls=%async_computation.6 | async-start | bytes 2621440 | tf_op jit(solution)/shard_map/reduce_scatter | solution.py:118
  112.4 7.4 %copy-start.12 = (bf16[8,32,4096]{2,1,0:T(8,128)(2,1)S(1)}, bf16[8,32,4096]{2,1,0:T(8,128)(2,1)}, u32[]{:S(2)}) copy-start(bf16[8,32,4096]{2,1,0:T(8,128)(2,1)} %all-gather.2.cloned.1.call-done) | copy-start | bytes 6291460
  112.4 15.5 %slice-start = ((s8[11534336]{0:T(1024)(128)(4,1)}), s8[4194304]{0:T(1024)(128)(4,1)S(1)}, s32[]{:S(2)}) async-start(s8[11534336]{0:T(1024)(128)(4,1)} %bitcast.72), calls=%async_computation.8 | async-start | bytes 8388608
  112.4 15.5 %slice-start.1 = ((s8[11534336]{0:T(1024)(128)(4,1)}), s8[4194304]{0:T(1024)(128)(4,1)S(1)}, s32[]{:S(2)}) async-start(s8[11534336]{0:T(1024)(128)(4,1)} %bitcast.72), calls=%async_computation.9 | async-start | bytes 8388608
  119.9 8.0 %slice-start.2 = ((s8[11534336]{0:T(1024)(128)(4,1)}), s8[3145728]{0:T(1024)(128)(4,1)S(1)}, s32[]{:S(2)}) async-start(s8[11534336]{0:T(1024)(128)(4,1)} %bitcast.72), calls=%async_computation.10 | async-start | bytes 6291456
  163.9 19.9 %all-to-all-start.1 = ((bf16[8,32,1024]{2,1,0:T(8,128)(2,1)}), bf16[8,32,1024]{2,1,0:T(8,128)(2,1)}, u32[]{:S(2)}, u32[]{:S(2)}) async-start(bf16[8,32,1024]{2,1,0:T(8,128)(2,1)} %reduce-scatter.5.cloned.1.call-done), calls=%async_computation.3 | async-start | bytes 1048576 | tf_op jit(solution)/shard_map/all_to_all | solution.py:121
  169.4 14.4 %copy-start.2 = (bf16[64,1024]{1,0:T(8,128)(2,1)S(1)}, bf16[64,1024]{1,0:T(8,128)(2,1)}, u32[]{:S(2)}) copy-start(bf16[64,1024]{1,0:T(8,128)(2,1)} %reduce-scatter.3.cloned.1.call-done) | copy-start | bytes 393220
Sparse Core Ops, SparseCore 0:
  41.0 22.5 reduce-scatter.2
  91.7 20.6 all-gather.1
  132.7 31.1 reduce-scatter.4
where the time goes:
time: 193 us; the launch traced here: 192 us
  waiting for transfers between devices  86.5 us (45%)
  blocking collectives  45.9 us (24%)
  matrix products  31.3 us (16%)
  between operations  14 us (7%)
  starting transfers between devices  5.63 us (3%)
  local copies, waits for them, and re-layouts  5.09 us (3%)
  other arithmetic  3.92 us (2%)
    reduce_scatter x1, waiting for transfers between devices, per_device(): lax.psum_scatter(partial_sum.astype(jnp.bfloat16), 'tp', scatter_dimensio...  31.3 us
    reduce_scatter x1, waiting for transfers between devices, per_device(): lax.psum_scatter(partial_out.astype(jnp.bfloat16), 'tp', scatter_dimensio...  21.7 us
    all_gather x1, waiting for transfers between devices, per_device(): lax.all_gather(lax.all_to_all(outbound, 'ep', split_axis=0, concat_axis=0...  20.8 us
    all_to_all x1, blocking collectives, per_device(): lax.all_to_all(outbound, 'ep', split_axis=0, concat_axis=0, tiled=True)  19.8 us
    all_to_all x1, waiting for transfers between devices, per_device(): lax.all_to_all(reduced, 'ep', split_axis=0, concat_axis=0, tiled=True)  12.7 us
    psum x1, blocking collectives, per_device(): squares = lax.psum(jnp.sum(source * source, axis=1), 'tp')  8.4 us
    dot_general x1, matrix products, per_device(): up_value = jnp.dot(flat_rows, w_up[0], preferred_element_type=jnp.float32)  8.01 us
    dot_general x1, matrix products, per_device(): jnp.dot(flat_rows, w_gate[0], preferred_element_type=jnp.float32)  7.42 us
  transfers between devices with their start and end apart: 4, of which 4 were waited for; matrix products, arithmetic and copies ran while one was open for 1% of the time, Pallas kernels for 0%

commit v1 on v0

--- a/solution.py
+++ b/solution.py
@@ -1,6 +1,10 @@
+import functools
+
 import jax
 import jax.numpy as jnp
 from jax import lax
+from jax.experimental import pallas as pl
+from jax.experimental.pallas import tpu as pltpu
 from jax.sharding import PartitionSpec as P
 
 GROUP_CH = 16
@@ -41,6 +45,314 @@
     return (jax.nn.gelu(output.reshape(batch_rows, -1)), jnp.stack([new_re, new_im], axis=1))
 
 
+MESH = pl.DeviceIdType.MESH
+
+
+def remote(src, dst, send_sem, recv_sem, target):
+    return pltpu.make_async_remote_copy(
+        src_ref=src,
+        dst_ref=dst,
+        send_sem=send_sem,
+        recv_sem=recv_sem,
+        device_id=target,
+        device_id_type=MESH,
+    )
+
+
+def enter(targets):
+    barrier = pltpu.get_barrier_semaphore()
+    for target in targets:
+        pl.semaphore_signal(barrier, inc=1, device_id=target, device_id_type=MESH)
+    pl.semaphore_wait(barrier, len(targets))
+
+
+def columns(place, width):
+    return pl.ds(pl.multiple_of(place * width, width), width)
+
+
+def branch_kernel(
+    chips,
+    part_ref,
+    resid_ref,
+    gain_ref,
+    after_ref,
+    normed_ref,
+    near,
+    staged,
+    far,
+    squares,
+    near_send,
+    near_recv,
+    far_send,
+    far_recv,
+    sq_send,
+    sq_recv,
+):
+    ep, tp = lax.axis_index("ep"), lax.axis_index("tp")
+    core, chip = lax.rem(tp, 2), lax.div(tp, 2)
+    width = resid_ref.shape[1]
+    members = 2 * chips
+    others = [lax.rem(chip + k, chips) for k in range(1, chips)]
+    peers = [lax.rem(tp + k, members) for k in range(1, members)]
+    partner = (ep, 2 * chip + 1 - core)
+    enter([(ep, p) for p in peers])
+    order = others + [chip]
+    first = []
+    for i, y in enumerate(order):
+        copy = remote(
+            part_ref.at[:, columns(2 * y + 1 - core, width)],
+            near.at[i],
+            near_send.at[i],
+            near_recv.at[i],
+            partner,
+        )
+        copy.start()
+        first.append(copy)
+    second = []
+    for i, y in enumerate(others):
+        first[i].wait_recv()
+        own = part_ref[:, columns(2 * y + core, width)].astype(jnp.float32)
+        staged[i] = (own + near[i].astype(jnp.float32)).astype(jnp.bfloat16)
+        copy = remote(staged.at[i], far.at[i], far_send.at[i], far_recv.at[i], (ep, 2 * y + core))
+        copy.start()
+        second.append(copy)
+    first[-1].wait_recv()
+    total = part_ref[:, columns(tp, width)].astype(jnp.float32)
+    total = total + near[chips - 1].astype(jnp.float32)
+    for i in range(chips - 1):
+        second[i].wait_recv()
+        total = total + far[i].astype(jnp.float32)
+    after = (resid_ref[...].astype(jnp.float32) + total).astype(jnp.bfloat16)
+    after_ref[...] = after
+    after = after.astype(jnp.float32)
+    own_sum = jnp.sum(after * after, axis=1, keepdims=True)
+    squares[0] = jnp.broadcast_to(own_sum, squares.shape[1:])
+    third = []
+    for k, p in enumerate(peers):
+        copy = remote(
+            squares.at[0], squares.at[k + 1], sq_send.at[k], sq_recv.at[k], (ep, p)
+        )
+        copy.start()
+        third.append(copy)
+    row_sum = squares[0]
+    for k in range(members - 1):
+        third[k].wait_recv()
+        row_sum = row_sum + squares[k + 1]
+    scale = lax.rsqrt(row_sum[:, :1] / (width * members) + epsilon)
+    normed_ref[...] = (after * scale * gain_ref[...]).astype(jnp.bfloat16)
+    for copy in first + second + third:
+        copy.wait_send()
+
+
+def dispatch_kernel(
+    chips,
+    out_ref_in,
+    rows_ref,
+    ep_send,
+    ep_recv,
+    pair_send,
+    pair_recv,
+    far_send,
+    far_recv,
+    relay_send,
+    relay_recv,
+):
+    ep, tp = lax.axis_index("ep"), lax.axis_index("tp")
+    experts, _, width = out_ref_in.shape
+    core, chip = lax.rem(tp, 2), lax.div(tp, 2)
+    others = [lax.rem(chip + k, chips) for k in range(1, chips)]
+    away = [lax.rem(ep + k, experts) for k in range(1, experts)]
+    partner = (ep, 2 * chip + 1 - core)
+    enter([(e, tp) for e in away] + [partner] + [(ep, 2 * y + core) for y in others])
+    mine = columns(tp, width)
+    sends = []
+    for k, e in enumerate(away):
+        copy = remote(
+            out_ref_in.at[e], rows_ref.at[ep, :, mine], ep_send.at[k], ep_recv.at[k], (e, tp)
+        )
+        copy.start()
+        sends.append(copy)
+    rows_ref[ep, :, mine] = out_ref_in[ep]
+    for k in range(experts):
+        source = lax.rem(ep + experts - k, experts)
+        if k == 0:
+            block = out_ref_in.at[ep]
+        else:
+            block = rows_ref.at[source, :, mine]
+            remote(block, block, ep_send.at[k - 1], ep_recv.at[k - 1], partner).wait_recv()
+        landing = rows_ref.at[source, :, mine]
+        for j, y in enumerate(others):
+            copy = remote(
+                block, landing, far_send.at[k, j], far_recv.at[k, j], (ep, 2 * y + core)
+            )
+            copy.start()
+            sends.append(copy)
+        copy = remote(block, landing, pair_send.at[k], pair_recv.at[k], partner)
+        copy.start()
+        sends.append(copy)
+    for k in range(experts):
+        source = lax.rem(ep + experts - k, experts)
+        for j in range(chips - 1):
+            y = lax.rem(chip + chips - 1 - j, chips)
+            block = rows_ref.at[source, :, columns(2 * y + core, width)]
+            remote(block, block, far_send.at[k, j], far_recv.at[k, j], partner).wait_recv()
+            copy = remote(block, block, relay_send.at[k, j], relay_recv.at[k, j], partner)
+            copy.start()
+            sends.append(copy)
+    for k in range(experts):
+        source = lax.rem(ep + experts - k, experts)
+        block = rows_ref.at[source, :, columns(2 * chip + 1 - core, width)]
+        remote(block, block, pair_send.at[k], pair_recv.at[k], partner).wait_recv()
+        for j in range(chips - 1):
+            y = lax.rem(chip + chips - 1 - j, chips)
+            block = rows_ref.at[source, :, columns(2 * y + 1 - core, width)]
+            remote(block, block, relay_send.at[k, j], relay_recv.at[k, j], partner).wait_recv()
+    for copy in sends:
+        copy.wait_send()
+
+
+def return_kernel(
+    chips,
+    part_ref,
+    back_ref,
+    near,
+    staged,
+    far,
+    summed,
+    near_send,
+    near_recv,
+    far_send,
+    far_recv,
+    ep_send,
+    ep_recv,
+):
+    ep, tp = lax.axis_index("ep"), lax.axis_index("tp")
+    experts, _, width = back_ref.shape
+    core, chip = lax.rem(tp, 2), lax.div(tp, 2)
+    others = [lax.rem(chip + k, chips) for k in range(1, chips)]
+    away = [lax.rem(ep + k, experts) for k in range(1, experts)]
+    targets = away + [ep]
+    partner = (ep, 2 * chip + 1 - core)
+    enter([(e, tp) for e in away] + [partner] + [(ep, 2 * y + core) for y in others])
+    order = others + [chip]
+    sends = []
+    for k, e in enumerate(targets):
+        for i, y in enumerate(order):
+            copy = remote(
+                part_ref.at[e, :, columns(2 * y + 1 - core, width)],
+                near.at[k, i],
+                near_send.at[k, i],
+                near_recv.at[k, i],
+                partner,
+            )
+            copy.start()
+            sends.append(copy)
+    for k, e in enumerate(targets):
+        for i, y in enumerate(others):
+            landed = near.at[k, i]
+            remote(landed, landed, near_send.at[k, i], near_recv.at[k, i], partner).wait_recv()
+            own = part_ref[e, :, columns(2 * y + core, width)].astype(jnp.float32)
+            staged[k, i] = (own + near[k, i].astype(jnp.float32)).astype(jnp.bfloat16)
+            copy = remote(
+                staged.at[k, i],
+                far.at[k, i],
+                far_send.at[k, i],
+                far_recv.at[k, i],
+                (ep, 2 * y + core),
+            )
+            copy.start()
+            sends.append(copy)
+    for k, e in enumerate(targets):
+        last = chips - 1
+        landed = near.at[k, last]
+        remote(landed, landed, near_send.at[k, last], near_recv.at[k, last], partner).wait_recv()
+        total = part_ref[e, :, columns(tp, width)].astype(jnp.float32)
+        total = total + near[k, last].astype(jnp.float32)
+        for i in range(last):
+            landed = far.at[k, i]
+            remote(landed, landed, far_send.at[k, i], far_recv.at[k, i], partner).wait_recv()
+            total = total + far[k, i].astype(jnp.float32)
+        if k == experts - 1:
+            back_ref[ep] = total.astype(jnp.bfloat16)
+        else:
+            summed[k] = total.astype(jnp.bfloat16)
+            copy = remote(
+                summed.at[k], back_ref.at[ep], ep_send.at[k], ep_recv.at[k], (e, tp)
+            )
+            copy.start()
+            sends.append(copy)
+    for k in range(1, experts):
+        landed = back_ref.at[lax.rem(ep + experts - k, experts)]
+        remote(landed, landed, ep_send.at[k - 1], ep_recv.at[k - 1], partner).wait_recv()
+    for copy in sends:
+        copy.wait_send()
+
+
+def call(kernel, out_shape, scratch, ident, name, *operands):
+    vmem = pl.BlockSpec(memory_space=pltpu.VMEM)
+    return pl.pallas_call(
+        kernel,
+        out_shape=out_shape,
+        in_specs=[vmem] * len(operands),
+        out_specs=jax.tree.map(lambda _: vmem, out_shape),
+        scratch_shapes=scratch,
+        compiler_params=pltpu.CompilerParams(collective_id=ident, has_side_effects=True),
+        name=name,
+    )(*operands)
+
+
+def sum_branch(partial_out, residual, gain, chips):
+    rows, width = residual.shape
+    dma = pltpu.SemaphoreType.DMA
+    shape = jax.ShapeDtypeStruct(residual.shape, jnp.bfloat16)
+    hops, peers = chips - 1, 2 * chips - 1
+    scratch = [
+        pltpu.VMEM((chips, rows, width), jnp.bfloat16),
+        pltpu.VMEM((hops, rows, width), jnp.bfloat16),
+        pltpu.VMEM((hops, rows, width), jnp.bfloat16),
+        pltpu.VMEM((2 * chips, rows, 128), jnp.float32),
+        dma((chips,)),
+        dma((chips,)),
+        dma((hops,)),
+        dma((hops,)),
+        dma((peers,)),
+        dma((peers,)),
+    ]
+    body = functools.partial(branch_kernel, chips)
+    return call(body, (shape, shape), scratch, 0, "sum_branch", partial_out, residual, gain)
+
+
+def dispatch_rows(outbound, chips):
+    experts, capacity, width = outbound.shape
+    dma = pltpu.SemaphoreType.DMA
+    hops = chips - 1
+    shape = jax.ShapeDtypeStruct((experts, capacity, width * 2 * chips), jnp.bfloat16)
+    scratch = [dma((experts - 1,))] * 2 + [dma((experts,))] * 2 + [dma((experts, hops))] * 4
+    body = functools.partial(dispatch_kernel, chips)
+    return call(body, shape, scratch, 1, "dispatch_rows", outbound)
+
+
+def return_rows(partial_sum, chips):
+    experts, capacity, full = partial_sum.shape
+    width, hops = full // (2 * chips), chips - 1
+    dma = pltpu.SemaphoreType.DMA
+    shape = jax.ShapeDtypeStruct((experts, capacity, width), jnp.bfloat16)
+    scratch = [
+        pltpu.VMEM((experts, chips, capacity, width), jnp.bfloat16),
+        pltpu.VMEM((experts, hops, capacity, width), jnp.bfloat16),
+        pltpu.VMEM((experts, hops, capacity, width), jnp.bfloat16),
+        pltpu.VMEM((experts - 1, capacity, width), jnp.bfloat16),
+        dma((experts, chips)),
+        dma((experts, chips)),
+        dma((experts, hops)),
+        dma((experts, hops)),
+        dma((experts - 1,)),
+        dma((experts - 1,)),
+    ]
+    body = functools.partial(return_kernel, chips)
+    return call(body, shape, scratch, 2, "return_rows", partial_sum)
+
+
 def per_device(
     residual,
     routes,
@@ -69,12 +381,11 @@
     experts_all = lax.axis_size("ep")
     seq_rows = residual.shape[0]
     capacity = 2 * seq_rows * TOPK // experts_all
-    source = residual.astype(jnp.float32)
-    squares = lax.psum(jnp.sum(source * source, axis=1), "tp")
-    own_gain = lax.dynamic_slice_in_dim(mix_gain, tp_place * shard_width, shard_width)
+    chips = lax.axis_size("tp") // 2
+    whole_rows = lax.all_gather(residual, "tp", axis=1, tiled=True).astype(jnp.float32)
+    squares = jnp.sum(whole_rows * whole_rows, axis=1)
     scale_rows = lax.rsqrt(squares / full_width + epsilon)[:, None]
-    outgoing = (source * scale_rows * own_gain).astype(jnp.bfloat16)
-    gathered = lax.all_gather(outgoing, "tp", axis=1, tiled=True)
+    gathered = (whole_rows * scale_rows * mix_gain).astype(jnp.bfloat16)
     u_in = jnp.dot(gathered, w_in, preferred_element_type=jnp.float32).astype(jnp.bfloat16)
     mixer_act, state_next = state_mixer(
         u_in, state_prev, decay_rate, rotation, log_step, in_re, in_im, read_re, read_im, skip_gain
@@ -84,14 +395,10 @@
     glu_logit = jnp.dot(all_channels, w_glu, preferred_element_type=jnp.float32)
     mixed = (mixer_act * jax.nn.sigmoid(glu_logit)).astype(jnp.bfloat16)
     partial_out = jnp.dot(mixed, w_out, preferred_element_type=jnp.float32)
-    branch = lax.psum_scatter(
-        partial_out.astype(jnp.bfloat16), "tp", scatter_dimension=1, tiled=True
-    ).astype(jnp.float32)
-    after_float = (source + branch).astype(jnp.bfloat16).astype(jnp.float32)
-    squares_ffn = lax.psum(jnp.sum(after_float * after_float, axis=1), "tp")
     ffn_own = lax.dynamic_slice_in_dim(ffn_gain, tp_place * shard_width, shard_width)
-    scale_ffn = lax.rsqrt(squares_ffn / full_width + epsilon)[:, None]
-    normed_ffn = (after_float * scale_ffn * ffn_own).astype(jnp.bfloat16)
+    after_mix, normed_ffn = sum_branch(
+        partial_out.astype(jnp.bfloat16), residual, ffn_own[None, :], chips
+    )
     flat_routes = routes.reshape(-1)
     onehot = (flat_routes[:, None] == jnp.arange(experts_all, dtype=jnp.int32)).astype(jnp.int32)
     before = jnp.cumsum(onehot, axis=0) - onehot
@@ -102,12 +409,7 @@
     combine_map = jnp.sum(jnp.where(matches, route_weights[:, :, None], 0.0), axis=1)
     outbound = jnp.einsum("bj,bd->jd", dispatch_map, normed_ffn, preferred_element_type=jnp.float32)
     outbound = outbound.astype(jnp.bfloat16).reshape(experts_all, capacity, shard_width)
-    arrived = lax.all_gather(
-        lax.all_to_all(outbound, "ep", split_axis=0, concat_axis=0, tiled=True),
-        "tp",
-        axis=2,
-        tiled=True,
-    )
+    arrived = dispatch_rows(outbound, chips)
     sources, slots_here, row_width = arrived.shape
     flat_rows = arrived.reshape(sources * slots_here, row_width)
     gate_value = jnp.dot(flat_rows, w_gate[0], preferred_element_type=jnp.float32)
@@ -115,13 +417,10 @@
     hidden = (jax.nn.silu(gate_value) * up_value).astype(jnp.bfloat16)
     partial_sum = jnp.dot(hidden, w_down[0], preferred_element_type=jnp.float32)
     partial_sum = partial_sum.reshape(sources, slots_here, row_width)
-    reduced = lax.psum_scatter(
-        partial_sum.astype(jnp.bfloat16), "tp", scatter_dimension=2, tiled=True
-    )
-    came_back = lax.all_to_all(reduced, "ep", split_axis=0, concat_axis=0, tiled=True)
+    came_back = return_rows(partial_sum.astype(jnp.bfloat16), chips)
     came_back = came_back.reshape(experts_all * capacity, shard_width).astype(jnp.float32)
     combined = jnp.dot(combine_map, came_back, precision=highest)
-    layer_out = (after_float + combined).astype(jnp.bfloat16)
+    layer_out = (after_mix.astype(jnp.float32) + combined).astype(jnp.bfloat16)
     return (layer_out, state_next)
 
 

time: 193 us -> 124 us (0.64)
  waiting for transfers between devices: 86.5 us -> 0 us
  Pallas kernels: 0 us -> 62.8 us
  blocking collectives: 45.9 us -> 14.5 us
  between operations: 14 us -> 0.93 us
  starting transfers between devices: 5.63 us -> 0 us
  matrix products: 31.3 us -> 34 us
    pallas_call x0 -> x3, Pallas kernels: none -> 62.8 us  [call(): pl.pallas_call(kernel, out_shape=out_shape, in_specs=[vmem] * len(operand...]
    reduce_scatter x2 -> x0, waiting for transfers between devices: 53 us -> none  [the longest x1 31.3 us: per_device(): lax.psum_scatter(partial_sum.astype(jnp.bfloat16), 'tp', scatter_dimensio...]
    all_gather x1 -> x0, waiting for transfers between devices: 20.8 us -> none  [per_device(): lax.all_gather(lax.all_to_all(outbound, 'ep', split_axis=0, concat_axis=0...]
    all_to_all x1 -> x0, blocking collectives: 19.8 us -> none  [per_device(): lax.all_to_all(outbound, 'ep', split_axis=0, concat_axis=0, tiled=True)]
    psum x2 -> x0, blocking collectives: 14.2 us -> none  [the longest x1 8.4 us: per_device(): squares = lax.psum(jnp.sum(source * source, axis=1), 'tp')]
    all_to_all x1 -> x0, waiting for transfers between devices: 12.7 us -> none  [per_device(): lax.all_to_all(reduced, 'ep', split_axis=0, concat_axis=0, tiled=True)]
    all_to_all x1 -> x0, starting transfers between devices: 5.51 us -> none  [per_device(): lax.all_to_all(reduced, 'ep', split_axis=0, concat_axis=0, tiled=True)]
    all_gather x1, blocking collectives: 6.5 us -> 8.87 us  [per_device(): lax.all_gather(residual, 'tp', axis=1, tiled=True).astype(jnp.float32)]
  transfers between devices with their start and end apart: 4 -> 0, of which waited for: 4 -> 0; matrix products, arithmetic and copies ran while one was open for 1% -> 0% of each run, Pallas kernels for 0% -> 0%
where the time goes in v1:
time: 124 us; the launch traced here: 123 us
  Pallas kernels  62.8 us (51%)
  matrix products  34 us (27%)
  blocking collectives  14.5 us (12%)
  local copies, waits for them, and re-layouts  6.46 us (5%)
  other arithmetic  4.29 us (3%)
    pallas_call x3, Pallas kernels, call(): pl.pallas_call(kernel, out_shape=out_shape, in_specs=[vmem] * len(operand...  62.8 us
    all_gather x1, blocking collectives, per_device(): lax.all_gather(residual, 'tp', axis=1, tiled=True).astype(jnp.float32)  8.87 us
    dot_general x1, matrix products, per_device(): jnp.dot(flat_rows, w_gate[0], preferred_element_type=jnp.float32)  8.71 us
    dot_general x1, matrix products, per_device(): up_value = jnp.dot(flat_rows, w_up[0], preferred_element_type=jnp.float32)  8.01 us
    all_gather x1, blocking collectives, per_device(): all_channels = lax.all_gather(mixer_bf, 'tp', axis=1, tiled=True)  5.6 us
    dot_general x1, matrix products, per_device(): partial_sum = jnp.dot(hidden, w_down[0], preferred_element_type=jnp.float32)  4.62 us
    unnamed x32, local copies, waits for them, and re-layouts  3 us
    dot_general x1, matrix products, per_device(): jnp.dot(gathered, w_in, preferred_element_type=jnp.float32)  2.79 us

profile of v1, /device:TPU:0, one launch (start us, length us, event | category | flops | bytes accessed | tf_op | source)
XLA Modules:
  0.0 123.0 jit_solution(9078385126284748873)
XLA Ops:
  0.6 0.8 exp.13
  1.5 1.3 %dynamic_slice.3 = f32[1024]{0:T(1024)} dynamic-slice(f32[4096]{0:T(1024)} %param.25, s32[]{:T(128)S(6)} %select_n.7), dynamic_slice_sizes={1024} | dynamic-slice | bytes 8196 | tf_op jit(solution)/shard_map/dynamic_slice | solution.py:398
  2.7 1.4 %add_divide_fusion = (f32[16,64]{1,0:T(8,128)S(1)}, f32[16,64]{1,0:T(8,128)S(1)}, f32[16,64]{1,0:T(8,128)}, f32[16,64]{1,0:T(8,128)}) fusion(f32[16,64]{1,0:T(8,128)} %param.28, f32[16,64]{1,0:T(8,128)} %param.27, f32[16]{0:T(128)S(1)} %exp.13), kind=kLoop, calls=%fused_computation.66 | loop fusion | flops 17408 | bytes 24640 | tf_op jit(solution)/shard_map/div | solution.py:30
  4.2 0.8 copy.61
  5.7 0.7 multiply_add_fusion.1
  6.4 1.4 %convert_reduce_fusion = (bf16[64,256]{1,0:T(8,128)(2,1)}, f32[64,256]{1,0:T(8,128)S(1)}) fusion(s32[64,2]{0,1:T(2,128)S(1)} %multiply_add_fusion.1, f32[64,2]{0,1:T(2,128)} %param.22), kind=kLoop, calls=%fused_computation.37 | loop fusion | flops 131072 | bytes 99328 | tf_op jit(solution)/shard_map/reduce_sum | solution.py:408
  7.9 8.9 %all_gather.6 = bf16[64,4096]{1,0:T(8,128)(2,1)S(1)} all-gather(bf16[64,1024]{1,0:T(8,128)(2,1)} %resid_ref.1), channel_id=1, replica_groups=mesh['ep'=8,'tp'=4] {'tp'}, dimensions={1}, use_global_device_ids=true | all-gather | bytes 655360 | tf_op jit(solution)/shard_map/all_gather | solution.py:385
  17.0 2.8 %convolution_convert_fusion.2 = bf16[64,256]{1,0:T(8,128)(2,1)} fusion(bf16[4096,256]{1,0:T(8,128)(2,1)} %param.26, bf16[64,4096]{1,0:T(8,128)(2,1)S(1)} %all_gather.6, f32[4096]{0:T(1024)} %param.24, f32[64]{0:T(128)S(1)} %add_rsqrt_fusion), kind=kOutput, calls=%fused_computation.28 | convolution fusion | flops 135282688 | bytes 2670848 | tf_op jit(solution)/shard_map/dot_general | solution.py:389
  19.8 0.9 copy.55
  21.4 0.7 fusion.15
  22.0 0.7 fusion.16
  22.7 0.9 fusion.58
  23.6 0.9 fusion.19
  24.7 5.6 %all_gather.7 = bf16[64,1024]{1,0:T(8,128)(2,1)S(1)} all-gather(bf16[64,256]{1,0:T(8,128)(2,1)S(1)} %fusion.52), channel_id=1, replica_groups=mesh['ep'=8,'tp'=4] {'tp'}, dimensions={1}, use_global_device_ids=true | all-gather | bytes 163840 | tf_op jit(solution)/shard_map/all_gather | solution.py:394
  30.3 2.6 %convolution_convert_fusion.part_ref = bf16[64,4096]{1,0:T(8,128)(2,1)} fusion(bf16[256,4096]{1,0:T(8,128)(2,1)S(1)} %copy-done, bf16[64,1024]{1,0:T(8,128)(2,1)S(1)} %all_gather.7, bf16[1024,256]{1,0:T(8,128)(2,1)} %param.35, f32[64,256]{1,0:T(8,128)S(1)} %copy.60), kind=kOutput, calls=%fused_computation.7 | convolution fusion | flops 168247296 | bytes 3342336 | tf_op jit(solution)/shard_map/dot_general | solution.py:397
  32.9 12.2 %sum_branch.1 = (bf16[64,1024]{1,0:T(8,128)(2,1)}, bf16[64,1024]{1,0:T(8,128)(2,1)}) custom-call(bf16[64,4096]{1,0:T(8,128)(2,1)} %convolution_convert_fusion.part_ref, bf16[64,1024]{1,0:T(8,128)(2,1)} %resid_ref.1, f32[1,1024]{1,0:T(1,128)} %bitcast.76), custom_call_target="tpu_custom_call" | custom-call | tf_op jit(solution)/shard_map/sum_branch/pallas_call | solution.py:293
  45.2 2.0 %convolution_convert_fusion.1 = bf16[256,1024]{1,0:T(8,128)(2,1)} fusion(bf16[64,1024]{1,0:T(8,128)(2,1)} %get-tuple-element.5, bf16[64,256]{1,0:T(8,128)(2,1)S(1)} %copy-done.8), kind=kOutput, calls=%fused_computation.12 | convolution fusion | flops 33816576 | bytes 688128 | tf_op jit(solution)/shard_map/bj,bd->jd/dot_general | solution.py:410
  47.3 1.6 %copy.63 = f32[64,2,16,64]{3,2,1,0:T(8,128)} copy(f32[64,2,16,64]{3,0,2,1:T(8,128)S(1)} %pad_maximum_fusion) | data formatting | bytes 1048576
  48.9 24.9 %dispatch_rows.1 = bf16[8,32,4096]{2,1,0:T(8,128)(2,1)} custom-call(bf16[8,32,1024]{2,1,0:T(8,128)(2,1)} %bitcast.70), custom_call_target="tpu_custom_call" | custom-call | tf_op jit(solution)/shard_map/dispatch_rows/pallas_call | solution.py:293
  73.8 8.7 %fusion.4 = f32[256,1408]{1,0:T(8,128)S(1)} fusion(bf16[256,4096]{1,0:T(8,128)(2,1)} %bitcast.68, bf16[1,4096,1408]{2,1,0:T(8,128)(2,1)} %param.37), kind=kOutput, calls=%fused_computation.4 | convolution fusion | flops 2952790016 | bytes 15073280 | tf_op jit(solution)/shard_map/dot_general | solution.py:415
  82.5 8.0 %fusion.12 = bf16[256,1408]{1,0:T(8,128)(2,1)S(1)} fusion(bf16[256,4096]{1,0:T(8,128)(2,1)S(1)} %bitcast.69, bf16[1,4096,1408]{2,1,0:T(8,128)(2,1)} %param.38, f32[256,1408]{1,0:T(8,128)S(1)} %fusion.4), kind=kOutput, calls=%fused_computation.9 | convolution fusion | flops 2954952704 | bytes 15794176 | tf_op jit(solution)/shard_map/dot_general | solution.py:416
  90.6 4.6 %fusion.6.part_ref = bf16[8,32,4096]{2,1,0:T(8,128)(2,1)} fusion(bf16[8,32,1408]{2,1,0:T(8,128)(2,1)S(1)} %bitcast.79, bf16[1,1408,4096]{2,1,0:T(8,128)(2,1)S(1)} %bitcast.78), kind=kOutput, calls=%fused_computation.6 | convolution fusion | flops 2953838592 | bytes 14352384 | tf_op jit(solution)/shard_map/dot_general | solution.py:418
  95.2 25.7 %return_rows.1 = bf16[8,32,1024]{2,1,0:T(8,128)(2,1)} custom-call(bf16[8,32,4096]{2,1,0:T(8,128)(2,1)} %fusion.6.part_ref), custom_call_target="tpu_custom_call" | custom-call | tf_op jit(solution)/shard_map/return_rows/pallas_call | solution.py:293
  120.9 2.1 %fusion.17 = bf16[64,1024]{1,0:T(8,128)(2,1)} fusion(f32[64,256]{1,0:T(8,128)S(1)} %get-tuple-element.15, bf16[256,1024]{1,0:T(8,128)(2,1)} %bitcast.71, bf16[64,1024]{1,0:T(8,128)(2,1)S(1)} %copy-done.7), kind=kOutput, calls=%fused_computation.18 | convolution fusion | flops 201523200 | bytes 851968 | tf_op jit(solution)/shard_map/dot_general | solution.py:422
  (43 shorter events, 1.9 us)
Async XLA Ops:
  0.6 29.7 %copy-start = (bf16[256,4096]{1,0:T(8,128)(2,1)S(1)}, bf16[256,4096]{1,0:T(8,128)(2,1)}, u32[]{:S(2)}) copy-start(bf16[256,4096]{1,0:T(8,128)(2,1)} %param.36) | copy-start | bytes 6291460
  5.3 15.3 %copy-start.2 = (f32[64,2,16,64]{3,2,1,0:T(8,128)S(1)}, f32[64,2,16,64]{3,2,1,0:T(8,128)}, u32[]{:S(2)}) copy-start(f32[64,2,16,64]{3,2,1,0:T(8,128)} %param.23) | copy-start | bytes 1572868
  16.9 3.8 %copy-start.3 = (f32[16,64,16]{1,2,0:T(8,128)S(1)}, f32[16,64,16]{1,2,0:T(8,128)}, u32[]{:S(2)}) copy-start(f32[16,64,16]{1,2,0:T(8,128)} %param.31) | copy-start | bytes 196612
  17.0 3.8 %copy-start.4 = (f32[16,64,16]{1,2,0:T(8,128)S(1)}, f32[16,64,16]{1,2,0:T(8,128)}, u32[]{:S(2)}) copy-start(f32[16,64,16]{1,2,0:T(8,128)} %param.30) | copy-start | bytes 196612
  20.6 0.7 copy-start.9
  20.6 0.7 copy-start.10
  20.7 1.9 %copy-start.6 = (f32[16,16,64]{2,1,0:T(8,128)S(1)}, f32[16,16,64]{2,1,0:T(8,128)}, u32[]{:S(2)}) copy-start(f32[16,16,64]{2,1,0:T(8,128)} %param.32) | copy-start | bytes 196612
  21.3 2.3 %copy-start.5 = (f32[16,16,64]{2,1,0:T(8,128)S(1)}, f32[16,16,64]{2,1,0:T(8,128)}, u32[]{:S(2)}) copy-start(f32[16,16,64]{2,1,0:T(8,128)} %param.33) | copy-start | bytes 196612
  21.3 2.3 %copy-start.11 = (f32[16,16]{1,0:T(8,128)S(1)}, f32[16,16]{1,0:T(8,128)}, u32[]{:S(2)}) copy-start(f32[16,16]{1,0:T(8,128)} %param.34) | copy-start | bytes 3076
  24.7 20.5 %copy-start.8 = (bf16[64,256]{1,0:T(8,128)(2,1)S(1)}, bf16[64,256]{1,0:T(8,128)(2,1)}, u32[]{:S(2)}) copy-start(bf16[64,256]{1,0:T(8,128)(2,1)} %get-tuple-element.14) | copy-start | bytes 98308
  73.8 8.8 %copy-start.1 = (bf16[8,32,4096]{2,1,0:T(8,128)(2,1)S(1)}, bf16[8,32,4096]{2,1,0:T(8,128)(2,1)}, u32[]{:S(2)}) copy-start(bf16[8,32,4096]{2,1,0:T(8,128)(2,1)} %dispatch_rows.1) | copy-start | bytes 6291460
  73.8 16.8 %slice-start = ((s8[11534336]{0:T(1024)(128)(4,1)}), s8[4194304]{0:T(1024)(128)(4,1)S(1)}, s32[]{:S(2)}) async-start(s8[11534336]{0:T(1024)(128)(4,1)} %bitcast.77), calls=%async_computation | async-start | bytes 8388608
  73.8 16.8 %slice-start.1 = ((s8[11534336]{0:T(1024)(128)(4,1)}), s8[4194304]{0:T(1024)(128)(4,1)S(1)}, s32[]{:S(2)}) async-start(s8[11534336]{0:T(1024)(128)(4,1)} %bitcast.77), calls=%async_computation.1 | async-start | bytes 8388608
  82.5 8.0 %slice-start.2 = ((s8[11534336]{0:T(1024)(128)(4,1)}), s8[3145728]{0:T(1024)(128)(4,1)S(1)}, s32[]{:S(2)}) async-start(s8[11534336]{0:T(1024)(128)(4,1)} %bitcast.77), calls=%async_computation.2 | async-start | bytes 6291456
  95.2 25.7 %copy-start.7 = (bf16[64,1024]{1,0:T(8,128)(2,1)S(1)}, bf16[64,1024]{1,0:T(8,128)(2,1)}, u32[]{:S(2)}) copy-start(bf16[64,1024]{1,0:T(8,128)(2,1)} %get-tuple-element.4) | copy-start | bytes 393220
